TPU v7x, 32 devices: a whole 2x2x4 slice. The times are simulated.
32 devices in a mesh: sp: 16 (over z, y, x), tp: 2 (over core).
Axes of the slice: x: 2, y: 2, z: 4, core: 2. Of those that a mesh axis runs over, the one named last changes fastest.
Arguments:
- hidden_in: bfloat16 [8192, 2048], P('sp'), may hold values from -64 to 64
- pre_gain: float32 [2048], replicated, may hold values from 0.1 to 1.9
- query_proj: bfloat16 [2048, 2048], P(None, 'tp'), may hold values from -2 to 2
- key_proj: bfloat16 [2048, 2048], P('sp', 'tp'), may hold values from -2 to 2
- value_proj: bfloat16 [2048, 2048], P('sp', 'tp'), may hold values from -0.125 to 0.125
- out_proj: bfloat16 [2048, 2048], P('tp'), may hold values from -0.125 to 0.125
- post_gain: float32 [2048], replicated, may hold values from 0.1 to 1.9
Outputs:
- layer_out: bfloat16 [8192, 2048], P(('sp', 'tp'))
- log_weight: float32 [32, 8192], P('tp', 'sp')
All inputs are finite; a program needn't handle non-finite values.
Results may differ from a plain program's by a relative error of at most 0.018.
The roundings to bfloat16 on the way count: a program that leaves them out, or rounds other values in their place, can miss the bound.
Values may be sent and summed in bfloat16 or wider, within the bound.
No kernel may reach another device: no remote copies, remote signals or barrier semaphores. Data moves between devices by JAX's collectives and lax.ppermute only.
A program may use at most 128 MiB of HBM per device.

v0:
```python
import jax
import jax.numpy as jnp
from jax import lax
from jax.sharding import PartitionSpec as P

HEAD_DIM = 64
SPAN = 128


EPS = 1e-06
ROPE_BASE = 10000.0
DILATIONS = (1, 4, 16)


def passed_along(value, axis, steps):
    count = lax.axis_size(axis)
    first, last = (max(0, -steps), min(count, count - steps))
    return lax.ppermute(value, axis, [(source, source + steps) for source in range(first, last)])


def rotate(vectors, positions):
    half_dim = vectors.shape[-1] // 2
    frequency = ROPE_BASE ** (-(jnp.arange(half_dim, dtype=jnp.float32) * 2.0 / vectors.shape[-1]))
    angles = positions[:, None] * frequency[None, :]
    cos_part = jnp.cos(angles)[:, None, :]
    sin_part = jnp.sin(angles)[:, None, :]
    front_half = vectors[..., :half_dim]
    back_half = vectors[..., half_dim:]
    return jnp.concatenate(
        [
            front_half * cos_part - back_half * sin_part,
            back_half * cos_part + front_half * sin_part,
        ],
        axis=-1,
    )


def rms_scale(matrix, gain):
    return matrix * lax.rsqrt(jnp.mean(matrix * matrix, axis=-1, keepdims=True) + EPS) * gain


def window_group(queries, buffer, dilation, offset):
    local_rows, head_count, head_depth = queries.shape
    reach_rows = dilation * SPAN
    start_row = buffer.shape[1] - local_rows - reach_rows
    key_rows = buffer[0, start_row:]
    value_rows = buffer[1, start_row:]
    res_len = local_rows // dilation
    block_len = min(SPAN, res_len)
    blocks = res_len // block_len
    query_blocks = queries.reshape(blocks, block_len, dilation, head_count, head_depth)
    key_res = key_rows.reshape(-1, dilation, head_count, head_depth)
    value_res = value_rows.reshape(-1, dilation, head_count, head_depth)
    width_keys = block_len + SPAN
    key_sets = jnp.stack(
        [
            key_res[block_idx * block_len : block_idx * block_len + width_keys]
            for block_idx in range(blocks)
        ]
    )
    value_sets = jnp.stack(
        [
            value_res[block_idx * block_len : block_idx * block_len + width_keys]
            for block_idx in range(blocks)
        ]
    )
    scores = jnp.einsum(
        "bqrhe,bkrhe->brhqk", query_blocks, key_sets, preferred_element_type=jnp.float32
    ) * head_depth ** (-0.5)
    query_idx = jnp.arange(block_len, dtype=jnp.int32)[:, None]
    key_idx = jnp.arange(width_keys, dtype=jnp.int32)[None, :]
    distance = query_idx + SPAN - key_idx
    in_band = (distance >= 0) & (distance <= SPAN)
    key_pos = (
        (
            jnp.arange(blocks, dtype=jnp.int32)[:, None, None, None, None] * block_len
            + jnp.arange(width_keys, dtype=jnp.int32)[None, None, None, None, :]
        )
        * dilation
        + jnp.arange(dilation, dtype=jnp.int32)[None, :, None, None, None]
        + (offset - reach_rows)
    )
    valid = in_band[None, None, None] & (key_pos >= 0)
    scores = jnp.where(valid, scores, -jnp.inf)
    row_max = jnp.max(scores, axis=-1, keepdims=True)
    exp_scores = jnp.exp(scores - row_max)
    denominator = jnp.sum(exp_scores, axis=-1, keepdims=True)
    levels = (row_max + jnp.log(denominator))[..., 0]
    shares = (exp_scores / denominator).astype(jnp.bfloat16)
    outcome = jnp.einsum(
        "brhqk,bkrhe->bqrhe", shares, value_sets, preferred_element_type=jnp.float32
    )
    outcome = outcome.reshape(local_rows, head_count, head_depth)
    levels = levels.transpose(2, 0, 3, 1).reshape(head_count, local_rows)
    return (outcome, levels)


def blend(group_outs, group_levels):
    levels = jnp.stack(group_levels)
    row_max = jnp.max(levels, axis=0)
    log_weight = row_max + jnp.log(jnp.sum(jnp.exp(levels - row_max[None]), axis=0))
    shares = jnp.exp(levels - log_weight[None])
    blended = jnp.sum(shares.transpose(0, 2, 1)[..., None] * jnp.stack(group_outs), axis=0)
    return (blended, log_weight)


def body(hidden_in, pre_gain, query_proj, key_proj, value_proj, out_proj, post_gain):
    local_rows = hidden_in.shape[0]
    local_width = query_proj.shape[1]
    head_count = local_width // HEAD_DIM
    normed = rms_scale(hidden_in.astype(jnp.float32), pre_gain).astype(jnp.bfloat16)
    offset = lax.axis_index("sp") * local_rows
    positions = (offset + jnp.arange(local_rows, dtype=jnp.int32)).astype(jnp.float32)
    queries = rotate(
        jnp.dot(normed, query_proj, preferred_element_type=jnp.float32).reshape(
            local_rows, head_count, HEAD_DIM
        ),
        positions,
    ).astype(jnp.bfloat16)
    pieces = (
        lax.all_gather(key_proj, "sp", axis=0, tiled=True),
        lax.all_gather(value_proj, "sp", axis=0, tiled=True),
    )
    key_sum = jnp.dot(normed, pieces[0], preferred_element_type=jnp.float32)
    value_sum = jnp.dot(normed, pieces[1], preferred_element_type=jnp.float32)
    key_rows = (
        rotate(key_sum.reshape(local_rows, head_count, HEAD_DIM), positions)
        .astype(jnp.bfloat16)
        .reshape(local_rows, local_width)
    )
    key_value = jnp.stack([key_rows, value_sum.astype(jnp.bfloat16)])
    behind = -(-(16 * SPAN) // local_rows)
    pieces = [passed_along(key_value, "sp", distance) for distance in range(behind, 0, -1)]
    buffer = jnp.concatenate(pieces + [key_value], axis=1)
    buffer = buffer.reshape(2, buffer.shape[1], head_count, HEAD_DIM)
    group_outs = []
    group_levels = []
    for dilation in DILATIONS:
        outcome, levels = window_group(queries, buffer, dilation, offset)
        group_outs.append(outcome)
        group_levels.append(levels)
    blended, log_weight = blend(group_outs, group_levels)
    attended = blended.astype(jnp.bfloat16).reshape(local_rows, local_width)
    summed = lax.psum_scatter(
        jnp.dot(attended, out_proj, preferred_element_type=jnp.float32).astype(jnp.bfloat16),
        "tp",
        scatter_dimension=0,
        tiled=True,
    ).astype(jnp.float32)
    layer_out = rms_scale(summed, post_gain).astype(jnp.bfloat16)
    return (layer_out, log_weight)


def solution(mesh):
    placed = (P("sp", None), P(), P(None, "tp"), P("sp", "tp"), P("sp", "tp"), P("tp", None), P())
    return jax.shard_map(
        body,
        mesh=mesh,
        in_specs=placed,
        out_specs=(P(("sp", "tp"), None), P("tp", "sp")),
        check_vma=False,
    )
```

profile of v0, /device:TPU:24, one launch (start us, length us, event | category | flops | bytes accessed | tf_op | source)
XLA Modules:
  0.0 568.6 jit_solution(712279927892896945)
XLA Ops:
  7.2 0.7 all-gather.3.cloned.1.call-update
  7.9 0.7 all-gather.5.cloned.1.call-update
  8.7 2.1 fusion.11
  11.2 5.3 fusion.78
  16.5 69.5 %all-gather.3.cloned.1.call-done = bf16[2048,1024]{1,0:T(8,128)(2,1)} async-done(((bf16[128,1024]{1,0:T(8,128)(2,1)}), bf16[2048,1024]{1,0:T(8,128)(2,1)}) %all-gather.3.cloned.1.call-update) | async-done | bytes 4194320 | tf_op jit(solution)/shard_map/all_gather | solution.py:121
  85.9 5.3 fusion.76
  91.2 1.6 subtract_convert_fusion.1
  93.5 69.4 %all-gather.5.cloned.1.call-done = bf16[2048,1024]{1,0:T(8,128)(2,1)} async-done(((bf16[128,1024]{1,0:T(8,128)(2,1)}), bf16[2048,1024]{1,0:T(8,128)(2,1)}) %all-gather.5.cloned.1.call-update) | async-done | bytes 4194320 | tf_op jit(solution)/shard_map/all_gather | solution.py:122
  162.9 5.2 fusion.51
  168.1 1.0 copy-done.8
  169.1 1.5 pad_maximum_fusion
  170.6 1.3 collective-permute-start
  171.9 3.4 collective-permute-start.1
  175.3 1.9 collective-permute-start.2
  177.3 2.1 collective-permute-start.3
  179.9 2.9 copy.102
  182.8 2.8 copy.104
  185.6 3.7 copy.101
  189.3 3.9 copy.103
  193.2 4.4 copy.110
  197.7 2.7 copy.111
  200.4 0.9 copy_bitcast_fusion.1
  201.3 0.9 copy_bitcast_fusion
  202.2 17.2 %collective-permute-done = bf16[2,512,1024]{2,1,0:T(8,128)(2,1)} collective-permute-done((bf16[2,512,1024]{2,1,0:T(8,128)(2,1)}, bf16[2,512,1024]{2,1,0:T(8,128)(2,1)}, u32[]{:S(2)}, u32[]{:S(2)}) %collective-permute-start) | collective-permute-done | bytes 2097184 | tf_op jit(solution)/shard_map/ppermute | solution.py:18
  219.4 3.2 constant_dynamic-update-slice_fusion.4
  222.6 42.7 %collective-permute-done.1 = bf16[2,512,1024]{2,1,0:T(8,128)(2,1)} collective-permute-done((bf16[2,512,1024]{2,1,0:T(8,128)(2,1)}, bf16[2,512,1024]{2,1,0:T(8,128)(2,1)}, u32[]{:S(2)}, u32[]{:S(2)}) %collective-permute-start.1) | collective-permute-done | bytes 2097184 | tf_op jit(solution)/shard_map/ppermute | solution.py:18
  265.4 3.1 constant_dynamic-update-slice_fusion.3
  268.5 42.3 %collective-permute-done.2 = bf16[2,512,1024]{2,1,0:T(8,128)(2,1)} collective-permute-done((bf16[2,512,1024]{2,1,0:T(8,128)(2,1)}, bf16[2,512,1024]{2,1,0:T(8,128)(2,1)}, u32[]{:S(2)}, u32[]{:S(2)}) %collective-permute-start.2) | collective-permute-done | bytes 2097184 | tf_op jit(solution)/shard_map/ppermute | solution.py:18
  310.8 3.1 constant_dynamic-update-slice_fusion.2
  313.9 42.2 %collective-permute-done.3 = bf16[2,512,1024]{2,1,0:T(8,128)(2,1)} collective-permute-done((bf16[2,512,1024]{2,1,0:T(8,128)(2,1)}, bf16[2,512,1024]{2,1,0:T(8,128)(2,1)}, u32[]{:S(2)}, u32[]{:S(2)}) %collective-permute-start.3) | collective-permute-done | bytes 2097184 | tf_op jit(solution)/shard_map/ppermute | solution.py:18
  356.1 3.1 constant_dynamic-update-slice_fusion.1
  359.2 1.6 constant_dynamic-update-slice_fusion
  360.8 13.8 %copy.99 = bf16[2,2560,1024]{1,2,0:T(8,128)(2,1)} copy(bf16[2,2560,1024]{2,1,0:T(8,128)(2,1)} %constant_dynamic-update-slice_fusion) | data formatting | bytes 20971520 | tf_op jit(solution)/shard_map/concatenate | solution.py:134
  374.6 9.2 %fusion.81 = (bf16[1,2560,1024]{2,1,0:T(8,128)(2,1)}, bf16[1,2560,1024]{2,1,0:T(8,128)(2,1)}) fusion(bf16[2,2560,1024]{2,1,0:T(8,128)(2,1)} %constant_dynamic-update-slice_fusion), kind=kLoop, calls=%fused_computation.140 | loop fusion | bytes 20971520 | tf_op jit(solution)/shard_map/slice | solution.py:46
  383.8 4.4 slice_bitcast_fusion.3
  388.2 5.0 fusion.80
  393.2 15.0 %reshape.505 = bf16[160,16,16,64]{3,2,1,0:T(8,128)(2,1)} reshape(bf16[1,2560,1024]{2,1,0:T(8,128)(2,1)} %get-tuple-element.14) | data formatting | bytes 10485760 | tf_op jit(solution)/shard_map/reshape.43
  408.2 18.8 %fusion.7 = (f32[16,16,32]{2,1,0:T(8,128)S(1)}, f32[16,16,32,160]{3,2,1,0:T(8,128)}) fusion(pred[16,32,160]{2,1,0:T(8,128)(4,1)S(1)} %broadcast_and_fusion, bf16[160,16,16,64]{3,2,1,0:T(8,128)(2,1)} %reshape.505, bf16[32,16,16,32]{3,0,2,1:T(8,128)(2,1)} %copy.111, bf16[32,16,16,32]{3,0,2,1:T(8,128)(2,1)S(1)} %copy-done), kind=kOutput, calls=%fused_computation.17 | convolution fusion | flops 173793280 | bytes 11649024 | tf_op jit(solution)/shard_map/bqrhe,bkrhe->brhqk/dot_general | solution.py:67
  427.0 5.2 fusion.10
  432.2 0.7 add_bitcast_fusion
  432.9 1.0 copy.113
  433.9 0.8 stack_reshape.34
  434.7 0.8 stack_reshape.30
  435.4 4.9 copy.105
  440.4 8.3 %fusion.6 = (f32[4,16,128]{2,1,0:T(8,128)S(1)}, f32[4,16,128,256]{3,2,1,0:T(8,128)S(1)}) fusion(pred[4,128,256]{2,1,0:T(8,128)(4,1)S(1)} %get-tuple-element.23, bf16[256,4,16,64]{3,2,1,0:T(8,128)(2,1)} %bitcast.111, bf16[128,4,16,32]{0,3,2,1:T(8,128)(2,1)S(1)} %copy-done.10, bf16[128,4,16,32]{0,3,2,1:T(8,128)(2,1)} %copy.103), kind=kOutput, calls=%fused_computation.16 | convolution fusion | flops 276815872 | bytes 11698176 | tf_op jit(solution)/shard_map/bqrhe,bkrhe->brhqk/dot_general | solution.py:67
  448.8 2.4 fusion.5
  451.2 0.8 copy-done.3
  452.0 7.0 %fusion.8 = (f32[4,16,128]{2,1,0:T(8,128)S(1)}, f32[4,16,128]{2,1,0:T(8,128)S(1)}) fusion(f32[4,16,128,256]{3,2,1,0:T(8,128)S(1)} %get-tuple-element.31, f32[4,16,128]{2,1,0:T(8,128)S(1)} %get-tuple-element.30, pred[4,128,256]{2,1,0:T(8,128)(4,1)S(1)} %get-tuple-element.22, f32[4,16,128]{2,1,0:T(8,128)S(1)} %get-tuple-element.28, ...), kind=kLoop, calls=%fused_computation.18 | loop fusion | flops 16760832 | bytes 17170432 | tf_op jit(solution)/shard_map/reduce_sum | solution.py:87
  459.1 0.6 copy.116
  460.4 5.1 copy.121
  466.1 9.0 %fusion.48 = f32[1,128,4,16,64]{1,4,3,2,0:T(8,128)S(1)} fusion(f32[4,16,128,256]{3,2,1,0:T(8,128)} %copy-done.3, f32[4,16,128]{2,1,0:T(8,128)} %copy-done.28, f32[4,16,128]{2,1,0:T(8,128)} %copy-done.25, pred[4,128,256]{2,1,0:T(8,128)(4,1)S(1)} %get-tuple-element.23, bf16[256,4,16,64]{3,2,1,0:T(8,128)(2,1)} %bitcast.110), kind=kOutput, calls=%fused_computation.64 | convolution fusion | flops 278921216 | bytes 12779520 | tf_op jit(solution)/shard_map/brhqk,bkrhe->bqrhe/dot_general | solution.py:90
  475.2 2.7 fusion.47
  478.0 2.7 copy.120
  481.5 4.5 copy.123
  486.0 5.8 %copy.126 = f32[1,512,16,64]{1,0,3,2:T(1,128)S(1)} copy(f32[1,512,16,64]{3,2,1,0:T(8,128)} %bitcast.107) | data formatting | bytes 4194304 | tf_op jit(solution)/shard_map/stack;reshape | solution.py:103
  491.8 14.4 %reshape.508 = bf16[160,16,16,64]{3,2,1,0:T(8,128)(2,1)} reshape(bf16[1,2560,1024]{2,1,0:T(8,128)(2,1)} %get-tuple-element.15) | data formatting | bytes 10485760 | tf_op jit(solution)/shard_map/reshape.68
  506.3 15.4 %fusion.25 = f32[1,32,16,16,64]{4,1,3,2,0:T(8,128)S(1)} fusion(bf16[160,16,16,64]{3,2,1,0:T(8,128)(2,1)} %reshape.508, f32[16,16,32,160]{3,2,1,0:T(8,128)} %get-tuple-element.27, f32[16,16,32]{2,1,0:T(8,128)S(1)} %fusion.10, f32[16,16,32]{2,1,0:T(8,128)S(1)} %get-tuple-element.26, pred[16,32,160]{2,1,0:T(8,128)(4,1)S(1)} %broadcast_and_fusion), kind=kOutput, calls=%fused_computation.40 | convolution fusion | flops 174325760 | bytes 12730368 | tf_op jit(solution)/shard_map/brhqk,bkrhe->bqrhe/dot_general | solution.py:90
  521.6 4.5 copy.125
  526.1 6.8 %copy.127 = f32[1,512,16,64]{1,0,3,2:T(1,128)} copy(f32[1,512,16,64]{3,2,1,0:T(8,128)} %bitcast.108) | data formatting | bytes 4194304 | tf_op jit(solution)/shard_map/stack;reshape | solution.py:103
  532.9 11.5 %fusion.4 = bf16[512,16,64]{0,2,1:T(8,128)(2,1)S(1)} fusion(f32[1,512,16,64]{1,0,3,2:T(1,128)} %copy.127, f32[1,512,16,64]{1,0,3,2:T(1,128)S(1)} %copy.126, f32[1,512,16,64]{1,0,3,2:T(1,128)} %bitcast.109, f32[3,512,16]{1,0,2:T(4,128)S(1)} %exponential_bitcast_fusion), kind=kLoop, calls=%fused_computation.5 | loop fusion | flops 5767168 | bytes 7438336 | tf_op jit(solution)/shard_map/reduce_sum | solution.py:103
  544.5 3.8 convolution_convert_fusion
  548.2 9.4 %reduce-scatter.2.cloned.1.call-done = bf16[256,2048]{1,0:T(8,128)(2,1)} async-done(((bf16[512,2048]{1,0:T(8,128)(2,1)}), bf16[256,2048]{1,0:T(8,128)(2,1)}) %reduce-scatter.2.cloned.1.call-update) | async-done | bytes 1048592 | tf_op jit(solution)/shard_map/reduce_scatter | solution.py:144
  557.6 1.5 fusion.28
  559.2 2.5 fusion.30
  (103 shorter events, 3.7 us)
Async XLA Ops:
  7.2 78.8 %all-gather.3.cloned.1.call-start = ((), (), s32[]{:S(2)}) async-start(), calls=%async_computation.1 | async-start | bytes 4456448 | tf_op jit(solution)/shard_map/all_gather | solution.py:121
  7.9 155.0 %all-gather.5.cloned.1.call-start = ((), (), s32[]{:S(2)}) async-start(), calls=%async_computation.2 | async-start | bytes 4456448 | tf_op jit(solution)/shard_map/all_gather | solution.py:122
  8.6 549.0 %reduce-scatter.2.cloned.1.call-start = ((), (), s32[]{:S(2)}) async-start(), calls=%async_computation.3 | async-start | bytes 3145728 | tf_op jit(solution)/shard_map/reduce_scatter | solution.py:144
  11.2 74.8 %copy-start.35 = (f32[2048]{0:T(1024)S(1)}, f32[2048]{0:T(1024)}, u32[]{:S(2)}) copy-start(f32[2048]{0:T(1024)} %param.8) | copy-start | bytes 24580
  168.1 1.0 copy-start.8
  170.6 48.8 %collective-permute-start = (bf16[2,512,1024]{2,1,0:T(8,128)(2,1)}, bf16[2,512,1024]{2,1,0:T(8,128)(2,1)}, u32[]{:S(2)}, u32[]{:S(2)}) collective-permute-start(bf16[2,512,1024]{2,1,0:T(8,128)(2,1)} %pad_maximum_fusion), channel_id=1, source_target_pairs={{0,8},{2,10},{4,12},{6,14},{8,16},{10,18},{12,20},{14,22},{16,24},... | collective-permute-start | bytes 6291464 | tf_op jit(solution)/shard_map/ppermute | solution.py:18
  171.9 93.4 %collective-permute-start.1 = (bf16[2,512,1024]{2,1,0:T(8,128)(2,1)}, bf16[2,512,1024]{2,1,0:T(8,128)(2,1)}, u32[]{:S(2)}, u32[]{:S(2)}) collective-permute-start(bf16[2,512,1024]{2,1,0:T(8,128)(2,1)} %pad_maximum_fusion), channel_id=1, source_target_pairs={{0,6},{2,8},{4,10},{6,12},{8,14},{10,16},{12,18},{14,20},{16,22},{... | collective-permute-start | bytes 6291464 | tf_op jit(solution)/shard_map/ppermute | solution.py:18
  175.3 135.4 %collective-permute-start.2 = (bf16[2,512,1024]{2,1,0:T(8,128)(2,1)}, bf16[2,512,1024]{2,1,0:T(8,128)(2,1)}, u32[]{:S(2)}, u32[]{:S(2)}) collective-permute-start(bf16[2,512,1024]{2,1,0:T(8,128)(2,1)} %pad_maximum_fusion), channel_id=1, source_target_pairs={{0,4},{2,6},{4,8},{6,10},{8,12},{10,14},{12,16},{14,18},{16,20},{1... | collective-permute-start | bytes 6291464 | tf_op jit(solution)/shard_map/ppermute | solution.py:18
  177.3 178.8 %collective-permute-start.3 = (bf16[2,512,1024]{2,1,0:T(8,128)(2,1)}, bf16[2,512,1024]{2,1,0:T(8,128)(2,1)}, u32[]{:S(2)}, u32[]{:S(2)}) collective-permute-start(bf16[2,512,1024]{2,1,0:T(8,128)(2,1)} %pad_maximum_fusion), channel_id=1, source_target_pairs={{0,2},{2,4},{4,6},{6,8},{8,10},{10,12},{12,14},{14,16},{16,18},{18... | collective-permute-start | bytes 6291464 | tf_op jit(solution)/shard_map/ppermute | solution.py:18
  193.2 7.1 %copy-start.7 = (bf16[512,16,32]{0,2,1:T(8,128)(2,1)S(1)}, bf16[512,16,32]{0,2,1:T(8,128)(2,1)}, u32[]{:S(2)}) copy-start(bf16[512,16,32]{0,2,1:T(8,128)(2,1)} %get-tuple-element.16) | copy-start | bytes 1572868
  193.2 8.1 %copy-start.6 = (bf16[512,16,32]{0,2,1:T(8,128)(2,1)S(1)}, bf16[512,16,32]{0,2,1:T(8,128)(2,1)}, u32[]{:S(2)}) copy-start(bf16[512,16,32]{0,2,1:T(8,128)(2,1)} %get-tuple-element.17) | copy-start | bytes 1572868
  268.4 90.7 %copy-start.9 = (bf16[1,512,1024]{2,1,0:T(8,128)(2,1)S(1)}, bf16[1,512,1024]{2,1,0:T(8,128)(2,1)}, u32[]{:S(2)}) copy-start(bf16[1,512,1024]{2,1,0:T(8,128)(2,1)} %copy-done.8) | copy-start | bytes 3145732
  393.2 15.0 %copy-start = (bf16[32,16,16,32]{3,0,2,1:T(8,128)(2,1)S(1)}, bf16[32,16,16,32]{3,0,2,1:T(8,128)(2,1)}, u32[]{:S(2)}) copy-start(bf16[32,16,16,32]{3,0,2,1:T(8,128)(2,1)} %copy.110) | copy-start | bytes 1572868
  427.0 8.4 %copy-start.5 = (bf16[1,1024,16,64]{1,3,2,0:T(8,128)(2,1)S(1)}, bf16[1,1024,16,64]{1,3,2,0:T(8,128)(2,1)}, u32[]{:S(2)}) copy-start(bf16[1,1024,16,64]{1,3,2,0:T(8,128)(2,1)} %get-tuple-element.13) | copy-start | bytes 6291460
  432.2 8.2 %copy-start.10 = (bf16[128,4,16,32]{0,3,2,1:T(8,128)(2,1)S(1)}, bf16[128,4,16,32]{0,3,2,1:T(8,128)(2,1)}, u32[]{:S(2)}) copy-start(bf16[128,4,16,32]{0,3,2,1:T(8,128)(2,1)} %copy.104) | copy-start | bytes 1572868
  440.3 8.4 %copy-start.15 = (bf16[1,256,1,16,64]{1,4,3,0,2:T(8,128)(2,1)S(1)}, bf16[1,256,1,16,64]{1,4,3,0,2:T(8,128)(2,1)}, u32[]{:S(2)}) copy-start(bf16[1,256,1,16,64]{1,4,3,0,2:T(8,128)(2,1)} %get-tuple-element.8) | copy-start | bytes 1572868
  440.3 8.4 %copy-start.16 = (bf16[1,256,1,16,64]{1,4,3,0,2:T(8,128)(2,1)S(1)}, bf16[1,256,1,16,64]{1,4,3,0,2:T(8,128)(2,1)}, u32[]{:S(2)}) copy-start(bf16[1,256,1,16,64]{1,4,3,0,2:T(8,128)(2,1)} %get-tuple-element.9) | copy-start | bytes 1572868
  440.3 8.4 %copy-start.17 = (bf16[1,256,1,16,64]{1,4,3,0,2:T(8,128)(2,1)S(1)}, bf16[1,256,1,16,64]{1,4,3,0,2:T(8,128)(2,1)}, u32[]{:S(2)}) copy-start(bf16[1,256,1,16,64]{1,4,3,0,2:T(8,128)(2,1)} %get-tuple-element.10) | copy-start | bytes 1572868
  440.3 8.4 %copy-start.18 = (bf16[1,256,1,16,64]{1,4,3,0,2:T(8,128)(2,1)S(1)}, bf16[1,256,1,16,64]{1,4,3,0,2:T(8,128)(2,1)}, u32[]{:S(2)}) copy-start(bf16[1,256,1,16,64]{1,4,3,0,2:T(8,128)(2,1)} %get-tuple-element.11) | copy-start | bytes 1572868
  440.3 8.4 %copy-start.19 = (bf16[4,128,16,32]{1,3,2,0:T(8,128)(2,1)S(1)}, bf16[4,128,16,32]{1,3,2,0:T(8,128)(2,1)}, u32[]{:S(2)}) copy-start(bf16[4,128,16,32]{1,3,2,0:T(8,128)(2,1)} %copy_bitcast_fusion.1) | copy-start | bytes 1572868
  440.4 8.4 %copy-start.20 = (bf16[4,128,16,32]{1,3,2,0:T(8,128)(2,1)S(1)}, bf16[4,128,16,32]{1,3,2,0:T(8,128)(2,1)}, u32[]{:S(2)}) copy-start(bf16[4,128,16,32]{1,3,2,0:T(8,128)(2,1)} %copy_bitcast_fusion) | copy-start | bytes 1572868
  448.7 3.3 copy-start.3
  448.7 16.7 %copy-start.25 = (f32[4,16,128]{2,1,0:T(8,128)}, f32[4,16,128]{2,1,0:T(8,128)S(1)}, u32[]{:S(2)}) copy-start(f32[4,16,128]{2,1,0:T(8,128)S(1)} %get-tuple-element.28) | copy-start | bytes 98308
  451.2 7.8 %copy-start.1 = (f32[4,16,128,256]{3,2,1,0:T(8,128)}, f32[4,16,128,256]{3,2,1,0:T(8,128)S(1)}, u32[]{:S(2)}) copy-start(f32[4,16,128,256]{3,2,1,0:T(8,128)S(1)} %get-tuple-element.31) | copy-start | bytes 25165828
  451.2 7.9 %copy-start.23 = (f32[4,16,128]{2,1,0:T(8,128)}, f32[4,16,128]{2,1,0:T(8,128)S(1)}, u32[]{:S(2)}) copy-start(f32[4,16,128]{2,1,0:T(8,128)S(1)} %get-tuple-element.30) | copy-start | bytes 98308
  452.0 8.3 %copy-start.4 = (bf16[1,1024,16,64]{1,3,2,0:T(8,128)(2,1)S(1)}, bf16[1,1024,16,64]{1,3,2,0:T(8,128)(2,1)}, u32[]{:S(2)}) copy-start(bf16[1,1024,16,64]{1,3,2,0:T(8,128)(2,1)} %get-tuple-element.12) | copy-start | bytes 6291460
  459.1 7.0 %copy-start.26 = (f32[4,16,128]{2,1,0:T(8,128)}, f32[4,16,128]{2,1,0:T(8,128)S(1)}, u32[]{:S(2)}) copy-start(f32[4,16,128]{2,1,0:T(8,128)S(1)} %get-tuple-element.32) | copy-start | bytes 98308
  459.1 7.0 %copy-start.28 = (f32[4,16,128]{2,1,0:T(8,128)}, f32[4,16,128]{2,1,0:T(8,128)S(1)}, u32[]{:S(2)}) copy-start(f32[4,16,128]{2,1,0:T(8,128)S(1)} %get-tuple-element.33) | copy-start | bytes 98308
  466.1 9.1 %copy-start.2 = (f32[4,16,128,256]{3,2,1,0:T(8,128)S(1)}, f32[4,16,128,256]{3,2,1,0:T(8,128)}, u32[]{:S(2)}) copy-start(f32[4,16,128,256]{3,2,1,0:T(8,128)} %copy-done.1) | copy-start | bytes 25165828
  466.1 9.1 %copy-start.11 = (bf16[1,256,1,16,64]{1,4,3,0,2:T(8,128)(2,1)S(1)}, bf16[1,256,1,16,64]{1,4,3,0,2:T(8,128)(2,1)}, u32[]{:S(2)}) copy-start(bf16[1,256,1,16,64]{1,4,3,0,2:T(8,128)(2,1)} %get-tuple-element.4) | copy-start | bytes 1572868
  466.1 9.1 %copy-start.12 = (bf16[1,256,1,16,64]{1,4,3,0,2:T(8,128)(2,1)S(1)}, bf16[1,256,1,16,64]{1,4,3,0,2:T(8,128)(2,1)}, u32[]{:S(2)}) copy-start(bf16[1,256,1,16,64]{1,4,3,0,2:T(8,128)(2,1)} %get-tuple-element.5) | copy-start | bytes 1572868
  466.1 9.1 %copy-start.13 = (bf16[1,256,1,16,64]{1,4,3,0,2:T(8,128)(2,1)S(1)}, bf16[1,256,1,16,64]{1,4,3,0,2:T(8,128)(2,1)}, u32[]{:S(2)}) copy-start(bf16[1,256,1,16,64]{1,4,3,0,2:T(8,128)(2,1)} %get-tuple-element.6) | copy-start | bytes 1572868
  466.1 9.1 %copy-start.14 = (bf16[1,256,1,16,64]{1,4,3,0,2:T(8,128)(2,1)S(1)}, bf16[1,256,1,16,64]{1,4,3,0,2:T(8,128)(2,1)}, u32[]{:S(2)}) copy-start(bf16[1,256,1,16,64]{1,4,3,0,2:T(8,128)(2,1)} %get-tuple-element.7) | copy-start | bytes 1572868
  466.1 9.1 %copy-start.24 = (f32[4,16,128]{2,1,0:T(8,128)S(1)}, f32[4,16,128]{2,1,0:T(8,128)}, u32[]{:S(2)}) copy-start(f32[4,16,128]{2,1,0:T(8,128)} %copy-done.23) | copy-start | bytes 98308
  466.1 9.1 %copy-start.27 = (f32[4,16,128]{2,1,0:T(8,128)S(1)}, f32[4,16,128]{2,1,0:T(8,128)}, u32[]{:S(2)}) copy-start(f32[4,16,128]{2,1,0:T(8,128)} %copy-done.26) | copy-start | bytes 98308
  477.9 2.8 copy-start.29
  478.0 3.1 copy-start.30
  478.0 3.1 copy-start.31
  478.0 3.1 copy-start.21
  478.0 3.1 copy-start.22
  481.4 10.5 %copy-start.32 = (f32[16,512]{1,0:T(8,128)}, f32[16,512]{1,0:T(8,128)S(1)}, u32[]{:S(2)}) copy-start(f32[16,512]{1,0:T(8,128)S(1)} %log_add_fusion) | copy-start | bytes 98308
  532.9 11.5 %copy-start.34 = (bf16[1024,2048]{1,0:T(8,128)(2,1)S(1)}, bf16[1024,2048]{1,0:T(8,128)(2,1)}, u32[]{:S(2)}) copy-start(bf16[1024,2048]{1,0:T(8,128)(2,1)} %param.12) | copy-start | bytes 12582916
  544.4 14.7 %copy-start.33 = (f32[2048]{0:T(1024)S(1)}, f32[2048]{0:T(1024)}, u32[]{:S(2)}) copy-start(f32[2048]{0:T(1024)} %param.13) | copy-start | bytes 24580
Sparse Core Ops, SparseCore 0:
  10.7 75.1 all-gather.2
  88.7 74.1 all-gather.4
  548.4 9.2 reduce-scatter.1
where the time goes:
time: 579 us; the launch traced here: 569 us
  waiting for transfers between devices  294 us (51%)
  local copies, waits for them, and re-layouts  137 us (24%)
  matrix products  76.2 us (13%)
  other arithmetic  37.1 us (6%)
  between operations  14.9 us (3%)
  starting transfers between devices  8.83 us (2%)
    ppermute x4, waiting for transfers between devices, passed_along(): lax.ppermute(value, axis, [(source, source + steps) for source in range(f...  145 us
    all_gather x1, waiting for transfers between devices, body(): lax.all_gather(key_proj, 'sp', axis=0, tiled=True)  69.5 us
    all_gather x1, waiting for transfers between devices, body(): lax.all_gather(value_proj, 'sp', axis=0, tiled=True)  69.4 us
    another operation x4, local copies, waits for them, and re-layouts  36 us
    dot_general x3, matrix products, window_group(): jnp.einsum('bqrhe,bkrhe->brhqk', query_blocks, key_sets, preferred_elemen...  29.6 us
    dot_general x3, matrix products, window_group(): jnp.einsum('brhqk,bkrhe->bqrhe', shares, value_sets, preferred_element_ty...  27.1 us
    concatenate x6, local copies, waits for them, and re-layouts, rotate(): jnp.concatenate([front_half * cos_part - back_half * sin_part, back_half...  15.7 us
    unnamed x76, local copies, waits for them, and re-layouts  14.4 us
  transfers between devices with their start and end apart: 7, of which 7 were waited for; matrix products, arithmetic and copies ran while one was open for 8% of the time, Pallas kernels for 0%

commit v1 on v0

v1 whole, which is shorter than its diff:
```python
import functools

import jax
import jax.numpy as jnp
from jax import lax
from jax.experimental import pallas as pl
from jax.experimental.pallas import tpu as pltpu
from jax.sharding import PartitionSpec as P

HEAD_DIM = 64
SPAN = 128
EPS = 1e-06
ROPE_BASE = 10000.0
DILATIONS = (1, 4, 16)
STEP = max(DILATIONS)
SUB = SPAN // STEP
NEG = -1e30
LANES = 128
F32 = jnp.float32
BF16 = jnp.bfloat16
SMEM = pl.BlockSpec(memory_space=pltpu.SMEM)
MIB = 1 << 20


def sds(shape, dtype):
    return jax.ShapeDtypeStruct(shape, dtype)


def lanes_of(width):
    return min(LANES, width)


def norm_body(hidden_ref, gain_ref, out_ref, scratch):
    rows = hidden_ref[...].astype(F32)
    mean = jnp.mean(rows * rows, axis=-1, keepdims=True)
    rows = rows * lax.rsqrt(mean + EPS) * gain_ref[...]
    for c in range(scratch.shape[0]):
        cols = slice(c * LANES, (c + 1) * LANES)
        scratch[c] = rows[:, cols]
        for r in range(0, STEP, 2):
            pair = [scratch[c, pl.ds(r + i, SUB, stride=STEP), :] for i in range(2)]
            out_ref[r * SUB : (r + 2) * SUB, cols] = jnp.concatenate(pair, axis=0).astype(BF16)


def norm_rows(hidden, gain):
    rows, width = hidden.shape
    return pl.pallas_call(
        norm_body,
        grid=(rows // SPAN,),
        in_specs=[
            pl.BlockSpec((SPAN, width), lambda i: (i, 0)),
            pl.BlockSpec((1, width), lambda i: (0, 0)),
        ],
        out_specs=pl.BlockSpec((SPAN, width), lambda i: (i, 0)),
        out_shape=sds((rows, width), BF16),
        scratch_shapes=[pltpu.VMEM((width // LANES, SPAN, LANES), F32)],
        compiler_params=pltpu.CompilerParams(vmem_limit_bytes=12 * MIB),
        name="norm_rows",
    )(hidden, gain.reshape(1, width))


def gather_body(idx, *refs):
    out_ref = refs[-1]
    for j, ref in enumerate(refs[:-1]):
        out_ref[idx[0] ^ j] = ref[...]


def gather_pieces(idx, pieces):
    return pl.pallas_call(
        gather_body,
        in_specs=[SMEM] + [pl.BlockSpec(memory_space=pltpu.VMEM)] * len(pieces),
        out_shape=sds((len(pieces),) + pieces[0].shape, pieces[0].dtype),
        compiler_params=pltpu.CompilerParams(vmem_limit_bytes=8 * MIB),
        name="gather_pieces",
    )(idx, *pieces)


def swap_halves(part):
    width = part.shape[-1]
    half = HEAD_DIM // 2
    if width == HEAD_DIM:
        return jnp.concatenate([part[:, half:], part[:, :half]], axis=-1)
    lane = lax.broadcasted_iota(jnp.int32, part.shape, 1)
    front = (lane & (HEAD_DIM - 1)) < half
    return jnp.where(front, pltpu.roll(part, width - half, 1), pltpu.roll(part, half, 1))


def rotated(rows, cos, sin):
    width = cos.shape[-1]
    parts = []
    for lo in range(0, rows.shape[-1], width):
        part = rows[:, lo : lo + width]
        parts.append(part * cos + swap_halves(part) * sin)
    return parts[0] if len(parts) == 1 else jnp.concatenate(parts, axis=-1)


def project_body(plan, local_rows, planes, idx, *refs):
    chunks = refs[: len(plan)]
    refs = refs[len(plan) :]
    own, ups, downs = refs[0], refs[1:planes], refs[planes : 2 * planes - 1]
    wq, cos_ref, sin_ref, q1, qr, k1, v1, kvr, wkv, scratch = refs[2 * planes - 1 :]
    place, plane, part = idx[0], idx[1], idx[2]
    depth = own.shape[0]
    width = wq.shape[1]

    def put(which, ref):
        wkv[pl.ds(pl.multiple_of(which * depth, depth), depth), :] = ref[...]

    put(plane, own)
    for k in range(1, planes):
        pl.when(plane >= k)(functools.partial(put, plane - k, ups[k - 1]))
        pl.when(plane + k < planes)(functools.partial(put, plane + k, downs[k - 1]))
    scale = HEAD_DIM**-0.5
    for j in sorted({entry[0] for entry in plan}):
        base = pl.multiple_of((place ^ j) * local_rows, local_rows)
        base_r = pl.multiple_of((place ^ j) * (local_rows // STEP), local_rows // STEP)
        for name, flat, split in (("q", q1, qr), ("k", k1, kvr.at[0]), ("v", v1, kvr.at[1])):
            for (jj, k, size, off), chunk in zip(plan, chunks):
                if jj != j:
                    continue
                weight = wq[...] if name == "q" else None
                if name == "k":
                    weight = wkv[:, :width]
                if name == "v":
                    weight = wkv[:, width:]
                rows = chunk.shape[0]
                at = 0 if size is None else pl.multiple_of((part ^ k) * size + off, rows)
                for lo in range(0, rows, 256):
                    few = min(256, rows - lo)
                    out = jnp.dot(chunk[lo : lo + few, :], weight, preferred_element_type=F32)
                    if name != "v":
                        table = pl.ds(pl.multiple_of(base + at + lo, few), few)
                        out = rotated(out, cos_ref[table, :], sin_ref[table, :])
                    if name == "q":
                        out = out * scale
                    scratch[pl.ds(pl.multiple_of(at + lo, few), few), :] = out
            flat[pl.ds(base, local_rows), :] = scratch[...].astype(BF16)
            for r in range(STEP):
                slabs = [
                    scratch[b * SPAN + r * SUB : b * SPAN + (r + 1) * SUB, :]
                    for b in range(local_rows // SPAN)
                ]
                split[r, pl.ds(base_r, local_rows // STEP), :] = jnp.concatenate(slabs, axis=0).astype(BF16)


def project(idx, plan, chunks, weights, wq, tables, local_rows, total):
    own, ups, downs = weights
    width = wq.shape[1]
    flat = sds((total, width), BF16)
    split = sds((STEP, total // STEP, width), BF16)
    count = len(chunks) + 1 + len(ups) + len(downs) + 3
    return pl.pallas_call(
        functools.partial(project_body, plan, local_rows, len(ups) + 1),
        in_specs=[SMEM] + [pl.BlockSpec(memory_space=pltpu.VMEM)] * count,
        out_shape=(flat, split, flat, flat, sds((2,) + split.shape, BF16)),
        scratch_shapes=[
            pltpu.VMEM((wq.shape[0], 2 * width), BF16),
            pltpu.VMEM((local_rows, width), F32),
        ],
        compiler_params=pltpu.CompilerParams(vmem_limit_bytes=48 * MIB),
        name="project",
    )(idx, *chunks, own, *ups, *downs, wq, *tables)


def steps_of(index, members, count, start):
    return ((index & (count - 1)) + start) * members + (index >> (count.bit_length() - 1))


def band(query_steps, key_steps):
    gap = query_steps - key_steps
    return jnp.where((gap >= 0) & (gap <= SPAN), 0.0, NEG).astype(F32)


def band_of(members, count, start):
    shape = (SPAN, members * count)
    query = steps_of(lax.broadcasted_iota(jnp.int32, shape, 0), members, SPAN // members, 0)
    return band(query, steps_of(lax.broadcasted_iota(jnp.int32, shape, 1), members, count, start))


def attend(query, keys, values, mask):
    width = query.shape[1]
    heads = width // HEAD_DIM
    group = lanes_of(width)
    per_group = group // HEAD_DIM
    owner = lax.broadcasted_iota(jnp.int32, query.shape, 1) >> (HEAD_DIM.bit_length() - 1)
    zero = jnp.zeros_like(query)
    stacked = [jnp.where(owner == h, query, zero) for h in range(heads)] if heads > 1 else [query]
    scores = lax.dot_general(
        jnp.concatenate(stacked, axis=0) if heads > 1 else query,
        keys,
        (((1,), (1,)), ((), ())),
        preferred_element_type=F32,
    )
    lane = lax.broadcasted_iota(jnp.int32, (SPAN, group), 1) >> (HEAD_DIM.bit_length() - 1)
    ones = jnp.ones((keys.shape[0], group), BF16)
    tops, sums, outs = [], [], []
    for g in range(heads // per_group):
        maxima, exps = [], []
        for h in range(g * per_group, (g + 1) * per_group):
            part = scores[h * SPAN : (h + 1) * SPAN, :] + mask
            top = jnp.max(part, axis=-1, keepdims=True)
            exps.append(jnp.exp(part - top).astype(BF16))
            maxima.append(jnp.broadcast_to(top, (SPAN, group)))
        exps = jnp.concatenate(exps, axis=0) if per_group > 1 else exps[0]
        mine = values[:, g * group : (g + 1) * group]
        if group == LANES:
            both = jnp.dot(exps, jnp.concatenate([mine, ones], axis=1), preferred_element_type=F32)
            out, total = both[:, :group], both[:, group:]
        else:
            out = jnp.dot(exps, mine, preferred_element_type=F32)
            total = jnp.dot(exps, ones, preferred_element_type=F32)

        def pick(parts):
            chosen = parts[0]
            for i in range(1, per_group):
                chosen = jnp.where(lane == i, parts[i], chosen)
            return chosen

        tops.append(pick(maxima))
        sums.append(pick([total[i * SPAN : (i + 1) * SPAN] for i in range(per_group)]))
        outs.append(pick([out[i * SPAN : (i + 1) * SPAN] for i in range(per_group)]))
    return [jnp.concatenate(x, axis=1) if len(x) > 1 else x[0] for x in (tops, sums, outs)]


def merged(old, new):
    top = jnp.maximum(old[0], new[0])
    keep, add = jnp.exp(old[0] - top), jnp.exp(new[0] - top)
    return [top, old[1] * keep + new[1] * add, old[2] * keep + new[2] * add]


def slabs_of(refs, members, first, stride, block, count):
    width = refs[0].shape[-1]
    return [
        jnp.concatenate(
            [
                ref[pl.ds(block, count), first + stride * a].reshape(count * SUB, width)
                for a in range(members)
            ],
            axis=0,
        )
        for ref in refs
    ]


def put_slabs(refs, values, members, first, stride, block, count):
    width = refs[0].shape[-1]
    for ref, value in zip(refs, values):
        for a in range(members):
            rows = value[a * count * SUB : (a + 1) * count * SUB, :]
            ref[pl.ds(block, count), first + stride * a] = rows.reshape(count, SUB, width)


def class_rows(ref, members, first, stride, start, count):
    parts = [ref[first + stride * a, pl.ds(start, count), :] for a in range(members)]
    return parts[0] if members == 1 else jnp.concatenate(parts, axis=0)


def local_body(q1, qr, k1, v1, kvr, top_ref, sum_ref, out_ref, mask_ref, half_ref):
    total, width = q1.shape
    blocks = total // SPAN
    state = (top_ref, sum_ref, out_ref)
    own = band_of(STEP, SUB, 0)
    half_ref[...] = own
    mask_ref[:, :SPAN] = band_of(STEP, SUB, -SUB)
    mask_ref[:, SPAN:] = own

    def write(block, values):
        for ref, value in zip(state, values):
            ref[block] = value.reshape(STEP, SUB, width)

    write(0, attend(q1[:SPAN, :], k1[:SPAN, :], v1[:SPAN, :], half_ref[...]))

    def near(block, carry):
        rows = pl.ds(pl.multiple_of(block * SPAN, SPAN), SPAN)
        behind = pl.ds(pl.multiple_of((block - 1) * SPAN, SPAN), 2 * SPAN)
        write(block, attend(q1[rows, :], k1[behind, :], v1[behind, :], mask_ref[...]))
        return carry

    lax.fori_loop(1, blocks, near, 0)
    for dilation in DILATIONS[1:]:
        members = STEP // dilation
        count = SPAN // members
        each = count // SUB
        half_ref[...] = band_of(members, count, 0)
        mask_ref[...] = band_of(members, 2 * count, -count)
        sets = blocks // each

        def first(res, carry):
            where = (members, res, dilation, 0, count)
            new = attend(
                class_rows(qr, *where),
                class_rows(kvr.at[0], *where),
                class_rows(kvr.at[1], *where),
                half_ref[...],
            )
            at = (members, res, dilation, 0, each)
            put_slabs(state, merged(slabs_of(state, *at), new), *at)
            return carry

        lax.fori_loop(0, dilation, first, 0)
        if sets == 1:
            continue

        def later(step, carry):
            res = step // (sets - 1)
            block = step - res * (sets - 1) + 1
            start = pl.multiple_of(block * count, count)
            behind = pl.multiple_of((block - 1) * count, count)
            new = attend(
                class_rows(qr, members, res, dilation, start, count),
                class_rows(kvr.at[0], members, res, dilation, behind, 2 * count),
                class_rows(kvr.at[1], members, res, dilation, behind, 2 * count),
                mask_ref[...],
            )
            at = (members, res, dilation, block * each, each)
            put_slabs(state, merged(slabs_of(state, *at), new), *at)
            return carry

        lax.fori_loop(0, dilation * (sets - 1), later, 0)


def attend_local(q1, qr, k1, v1, kvr):
    total, width = q1.shape
    state = sds((total // SPAN, STEP, SUB, width), F32)
    return pl.pallas_call(
        local_body,
        in_specs=[pl.BlockSpec(memory_space=pltpu.VMEM)] * 5,
        out_shape=(state,) * 3,
        scratch_shapes=[pltpu.VMEM((SPAN, 2 * SPAN), F32), pltpu.VMEM((SPAN, SPAN), F32)],
        compiler_params=pltpu.CompilerParams(vmem_limit_bytes=32 * MIB),
        name="attend_local",
    )(q1, qr, k1, v1, kvr)


def halo_body(idx, q1, qr, halo, top_in, sum_in, out_in, att_ref, level_ref, top_ref, sum_ref, out_ref, half_ref, near_ref, turn, turn_level):
    total, width = q1.shape
    blocks = total // SPAN
    group = lanes_of(width)
    groups = width // group
    state = (top_ref, sum_ref, out_ref)
    given = (top_in, sum_in, out_in)
    for ref, source in zip(state, given):
        ref[...] = source[...]

    @pl.when(idx[1] > 0)
    def _():
        pair = 2 * SUB
        near_ref[...] = band_of(STEP, pair, -pair)
        last = total // STEP
        new = attend(
            q1[:SPAN, :],
            class_rows(halo.at[0], STEP, 0, 1, last - pair, pair),
            class_rows(halo.at[1], STEP, 0, 1, last - pair, pair),
            near_ref[...],
        )
        old = [ref[0].reshape(SPAN, width) for ref in state]
        for ref, value in zip(state, merged(old, new)):
            ref[0] = value.reshape(STEP, SUB, width)
        for dilation in DILATIONS[1:]:
            members = STEP // dilation
            count = SPAN // members
            each = count // SUB
            half_ref[...] = band_of(members, count, -count)

            def first(res, carry):
                where = (members, res, dilation, last - count, count)
                new = attend(
                    class_rows(qr, members, res, dilation, 0, count),
                    class_rows(halo.at[0], *where),
                    class_rows(halo.at[1], *where),
                    half_ref[...],
                )
                at = (members, res, dilation, 0, each)
                put_slabs(state, merged(slabs_of(state, *at), new), *at)
                return carry

            lax.fori_loop(0, dilation, first, 0)

    spread = att_ref.shape[1] // SPAN
    for block in range(blocks):
        top, denominator, out = [ref[block].reshape(SPAN, width) for ref in state]
        level = top + jnp.log(denominator)
        out = out / denominator
        for g in range(groups):
            turn[g, :, :group] = out[:, g * group : (g + 1) * group]
        chosen = level[:, :group]
        lane = lax.broadcasted_iota(jnp.int32, (SPAN, group), 1)
        for g in range(1, groups):
            chosen = jnp.where((lane & (HEAD_DIM - 1)) == g, level[:, g * group : (g + 1) * group], chosen)
        turn_level[:, :group] = chosen
        place, low = block // spread, (block % spread) * SPAN
        rows = []
        for m in range(SUB):
            here = slice(low + m * STEP, low + (m + 1) * STEP)
            for g in range(groups):
                spun = turn[g, pl.ds(m, STEP, stride=SUB), :]
                att_ref[place, here, g * group : (g + 1) * group] = spun[:, :group].astype(BF16)
            rows.append(turn_level[pl.ds(m, STEP, stride=SUB), :])
        flipped = jnp.concatenate(rows, axis=0).T
        for h in range(width // HEAD_DIM):
            source = (h % (group // HEAD_DIM)) * HEAD_DIM + h // (group // HEAD_DIM)
            level_ref[place, h : h + 1, low : low + SPAN] = flipped[source : source + 1, :]


def attend_halo(idx, q1, qr, halo, state, places):
    total, width = q1.shape
    local_rows = total // places
    group = lanes_of(width)
    full = pltpu.VMEM(state[0].shape, F32)
    return pl.pallas_call(
        halo_body,
        in_specs=[SMEM] + [pl.BlockSpec(memory_space=pltpu.VMEM)] * 6,
        out_shape=(
            sds((places, local_rows, width), BF16),
            sds((places, width // HEAD_DIM, local_rows), F32),
        ),
        scratch_shapes=[
            full,
            full,
            full,
            pltpu.VMEM((SPAN, SPAN), F32),
            pltpu.VMEM((SPAN, 2 * SPAN), F32),
            pltpu.VMEM((width // group, SPAN, LANES), F32),
            pltpu.VMEM((SPAN, LANES), F32),
        ],
        compiler_params=pltpu.CompilerParams(vmem_limit_bytes=40 * MIB),
        name="attend_halo",
    )(idx, q1, qr, halo, *state)


def out_body(idx, *refs):
    parts = refs[-1].shape[0]
    weight, out_ref = refs[-2], refs[-1]
    pieces = refs[:-2]
    rows, width = out_ref.shape[1], pieces[0].shape[1]
    for k in range(parts):
        at = pl.ds(pl.multiple_of((idx[2] ^ k) * rows, rows), rows)
        total = None
        for j, piece in enumerate(pieces):
            mine = weight[pl.ds(pl.multiple_of((idx[0] ^ j) * width, width), width), :]
            term = jnp.dot(piece[at, :], mine, preferred_element_type=F32)
            total = term if total is None else total + term
        out_ref[k] = total.astype(BF16)


def out_partials(idx, pieces, weight, parts):
    rows, width = pieces[0].shape
    depth, wide = weight.shape
    tile = min(512, wide)
    return pl.pallas_call(
        out_body,
        grid=(wide // tile,),
        in_specs=[SMEM]
        + [pl.BlockSpec((rows, width), lambda i: (0, 0))] * len(pieces)
        + [pl.BlockSpec((depth, tile), lambda i: (0, i))],
        out_specs=pl.BlockSpec((parts, rows // parts, tile), lambda i: (0, 0, i)),
        out_shape=sds((parts, rows // parts, wide), BF16),
        compiler_params=pltpu.CompilerParams(vmem_limit_bytes=16 * MIB),
        name="out_partials",
    )(idx, *pieces, weight)


def final_body(*refs):
    gain_ref, out_ref = refs[-2], refs[-1]
    summed = refs[0][...].astype(F32)
    for ref in refs[1:-2]:
        summed = summed + ref[...].astype(F32)
    mean = jnp.mean(summed * summed, axis=-1, keepdims=True)
    out_ref[...] = (summed * lax.rsqrt(mean + EPS) * gain_ref[...]).astype(BF16)


def final_norm(pieces, gain):
    rows, width = pieces[0].shape
    tile = min(128, rows)
    block = pl.BlockSpec((tile, width), lambda i: (i, 0))
    return pl.pallas_call(
        final_body,
        grid=(rows // tile,),
        in_specs=[block] * len(pieces) + [pl.BlockSpec((1, width), lambda i: (0, 0))],
        out_specs=block,
        out_shape=sds((rows, width), BF16),
        compiler_params=pltpu.CompilerParams(vmem_limit_bytes=16 * MIB),
        name="final_norm",
    )(*pieces, gain.reshape(1, width))


def body(hidden_in, pre_gain, query_proj, key_proj, value_proj, out_proj, post_gain):
    local_rows, model = hidden_in.shape
    devices, parts = lax.axis_size("sp"), lax.axis_size("tp")
    heads = query_proj.shape[1] // HEAD_DIM
    places = STEP * SPAN // local_rows
    if places < 1 or devices % places or heads % places or local_rows % SPAN:
        raise ValueError("unsupported split")
    planes = devices // places
    total = places * local_rows
    width = heads // places * HEAD_DIM
    index, part = lax.axis_index("sp"), lax.axis_index("tp")
    place, plane = index % places, index // places
    idx = jnp.stack([place, plane, part]).astype(jnp.int32)

    def across(value, j):
        return lax.ppermute(value, "sp", [(s, s ^ j) for s in range(devices)])

    def upward(value, sign=1):
        moves = [(s, s + sign * places) for s in range(devices)]
        return lax.ppermute(value, "sp", [m for m in moves if 0 <= m[1] < devices])

    def partner(value, k):
        return lax.ppermute(value, "tp", [(s, s ^ k) for s in range(parts)])

    def columns(j):
        at = (place ^ j) * width
        size = (key_proj.shape[0], width)
        return jnp.concatenate([lax.dynamic_slice(w, (0, at), size) for w in (key_proj, value_proj)], axis=1)

    pieces = [columns(0)] + [across(columns(j), j) for j in range(1, places)]
    own = gather_pieces(idx, pieces).reshape(places * key_proj.shape[0], 2 * width)
    ups, downs = [], []
    for k in range(1, planes):
        ups.append(upward(ups[-1] if ups else own, 1))
        downs.append(upward(downs[-1] if downs else own, -1))

    normed = norm_rows(hidden_in, pre_gain)
    size = local_rows // parts
    mine = lax.dynamic_slice(normed, (part * size, 0), (size, model))
    arrived = []
    if places == 4:
        one, two = across(mine, 1), across(mine, 2)
        half = size // 2
        arrived = [(1, 0, one), (2, 0, two), (3, 0, across(two[:half], 1)), (3, half, across(one[half:], 2))]
    else:
        arrived = [(j, 0, across(mine, j)) for j in range(1, places)]
    plan, chunks = [(0, 0, None, 0)], [normed]
    for j, off, rows in arrived:
        for k in range(parts):
            plan.append((j, k, size, off))
            chunks.append(rows if k == 0 else partner(rows, k))

    wide = lanes_of(width)
    token = jnp.arange(total, dtype=jnp.int32).reshape(total // SPAN, SUB, STEP).transpose(0, 2, 1).reshape(total)
    positions = (plane * total + token).astype(F32)
    lane = jnp.arange(wide, dtype=jnp.int32) % HEAD_DIM
    half_dim = HEAD_DIM // 2
    frequency = ROPE_BASE ** (-((lane % half_dim).astype(F32) * 2.0 / HEAD_DIM))
    angles = positions[:, None] * frequency[None, :]
    tables = (jnp.cos(angles), jnp.sin(angles) * jnp.where(lane < half_dim, -1.0, 1.0)[None, :])

    wq = lax.dynamic_slice(query_proj, (0, place * width), (model, width))
    q1, qr, k1, v1, kvr = project(idx, tuple(plan), chunks, (own, ups, downs), wq, tables, local_rows, total)
    halo = upward(kvr)
    state = attend_local(q1, qr, k1, v1, kvr)
    attended, levels = attend_halo(idx, q1, qr, halo, state, places)

    def swapped(value):
        slices = [lax.dynamic_index_in_dim(value, place ^ j, 0, keepdims=False) for j in range(places)]
        return [slices[0]] + [across(slices[j], j) for j in range(1, places)]

    partials = out_partials(idx, swapped(attended), out_proj, parts)
    log_weight = gather_pieces(idx, swapped(levels)).reshape(heads, local_rows)
    layer_out = final_norm([partials[0]] + [partner(partials[k], k) for k in range(1, parts)], post_gain)
    return (layer_out, log_weight)


def solution(mesh):
    placed = (P("sp", None), P(), P(None, "tp"), P("sp", "tp"), P("sp", "tp"), P("tp", None), P())
    return jax.shard_map(
        body,
        mesh=mesh,
        in_specs=placed,
        out_specs=(P(("sp", "tp"), None), P("tp", "sp")),
        check_vma=False,
    )
```

time: 579 us -> 192 us (0.33); the launches traced: 569 us -> 191 us
  waiting for transfers between devices: 294 us -> 71.5 us
  local copies, waits for them, and re-layouts: 137 us -> 18 us
  matrix products: 76.2 us -> 0 us
  Pallas kernels: 0 us -> 60.2 us
  other arithmetic: 37.1 us -> 5.75 us
  starting transfers between devices: 8.83 us -> 34.7 us
  between operations: 14.9 us -> 0.93 us
    all_gather x2 -> x0, waiting for transfers between devices: 139 us -> none  [the longest x1 69.5 us: body(): lax.all_gather(key_proj, 'sp', axis=0, tiled=True)]
    dot_general x10 -> x0, matrix products: 76.2 us -> none  [the longest x3 29.6 us: window_group(): jnp.einsum('bqrhe,bkrhe->brhqk', query_blocks, key_sets, preferred_elemen...]
    ppermute x4 -> x25, waiting for transfers between devices: 145 us -> 71.5 us  [the longest x13 37.7 us: across(): return lax.ppermute(value, 'sp', [(s, s ^ j) for s in range(devices)])]
    pallas_call x0 -> x8, Pallas kernels: none -> 60.2 us  [the longest x1 24.8 us: attend_local(): pl.pallas_call(local_body, in_specs=[pl.BlockSpec(memory_space=pltpu.VMEM...]
    another operation x11 -> x0, local copies, waits for them, and re-layouts: 54.7 us -> none
    concatenate x7 -> x0, local copies, waits for them, and re-layouts: 29.5 us -> none  [the longest x6 15.7 us: rotate(): jnp.concatenate([front_half * cos_part - back_half * sin_part, back_half...]
    reduce_sum x6 -> x0, other arithmetic: 27.5 us -> none  [the longest x2 12.2 us: window_group(): denominator = jnp.sum(exp_scores, axis=-1, keepdims=True)]
    ppermute x4 -> x25, starting transfers between devices: 8.71 us -> 34.7 us  [the longest x7 17.3 us: upward(): return lax.ppermute(value, 'sp', [m for m in moves if 0 <= m[1] < devices])]
  transfers between devices with their start and end apart: 7 -> 25, of which waited for: 7 -> 14; matrix products, arithmetic and copies ran while one was open for 8% -> 7% of each run, Pallas kernels for 0% -> 14%
where the time goes in v1:
time: 192 us; the launch traced here: 191 us
  waiting for transfers between devices  71.5 us (37%)
  Pallas kernels  60.2 us (31%)
  starting transfers between devices  34.7 us (18%)
  local copies, waits for them, and re-layouts  18 us (9%)
  other arithmetic  5.75 us (3%)
    ppermute x13, waiting for transfers between devices, across(): return lax.ppermute(value, 'sp', [(s, s ^ j) for s in range(devices)])  37.7 us
    ppermute x7, waiting for transfers between devices, upward(): return lax.ppermute(value, 'sp', [m for m in moves if 0 <= m[1] < devices])  33.8 us
    pallas_call x1, Pallas kernels, attend_local(): pl.pallas_call(local_body, in_specs=[pl.BlockSpec(memory_space=pltpu.VMEM...  24.8 us
    ppermute x7, starting transfers between devices, upward(): return lax.ppermute(value, 'sp', [m for m in moves if 0 <= m[1] < devices])  17.3 us
    ppermute x13, starting transfers between devices, across(): return lax.ppermute(value, 'sp', [(s, s ^ j) for s in range(devices)])  16.8 us
    pallas_call x1, Pallas kernels, project(): pl.pallas_call(functools.partial(project_body, plan, local_rows, len(ups)...  14.2 us
    pallas_call x1, Pallas kernels, attend_halo(): pl.pallas_call(halo_body, in_specs=[SMEM] + [pl.BlockSpec(memory_space=pl...  12.5 us
    unnamed x28, local copies, waits for them, and re-layouts  8.8 us
  transfers between devices with their start and end apart: 25, of which 14 were waited for; matrix products, arithmetic and copies ran while one was open for 7% of the time, Pallas kernels for 14%

profile of v1, /device:TPU:24, one launch (start us, length us, event | category | flops | bytes accessed | tf_op | source)
XLA Modules:
  0.0 191.1 jit_solution(4885813985831443419)
XLA Ops:
  0.6 1.6 copy-done.7
  2.2 0.7 copy-done.10
  2.9 2.4 %norm_rows.1.refs_0_ = bf16[512,2048]{1,0:T(8,128)(2,1)S(1)} custom-call(bf16[512,2048]{1,0:T(8,128)(2,1)S(1)} %copy-done.7, f32[1,2048]{1,0:T(1,128)S(1)} %bitcast.29), custom_call_target="tpu_custom_call" | custom-call | tf_op jit(solution)/shard_map/norm_rows/pallas_call | solution.py:47
  5.3 0.0 copy-start.12
  5.3 0.0 copy-start.13
  5.4 1.0 constant_dynamic-slice_fusion.9
  6.4 1.5 collective-permute-start.2
  7.9 1.5 collective-permute-start
  9.4 0.1 constant_dynamic-slice_fusion.1
  9.5 0.6 collective-permute-start.9
  10.1 0.6 collective-permute-start.8
  10.7 2.5 %collective-permute-start.10 = (bf16[128,512]{1,0:T(8,128)(2,1)S(1)}, bf16[128,512]{1,0:T(8,128)(2,1)S(1)}, u32[]{:S(2)}, u32[]{:S(2)}) collective-permute-start(bf16[128,512]{1,0:T(8,128)(2,1)S(1)} %pad_maximum_fusion.3), channel_id=1, source_target_pairs={{0,6},{2,4},{4,2},{6,0},{8,14},{10,12},{12,10},{14,8},{16,22},{18,... | collective-permute-start | bytes 393224 | tf_op jit(solution)/shard_map/ppermute | solution.py:502
  13.2 0.1 pad_add_fusion.idx
  13.3 21.2 %collective-permute-done.9.refs_2_ = bf16[128,512]{1,0:T(8,128)(2,1)S(1)} collective-permute-done((bf16[128,512]{1,0:T(8,128)(2,1)S(1)}, bf16[128,512]{1,0:T(8,128)(2,1)S(1)}, u32[]{:S(2)}, u32[]{:S(2)}) %collective-permute-start.9) | collective-permute-done | bytes 131104 | tf_op jit(solution)/shard_map/ppermute | solution.py:502
  34.5 2.4 %collective-permute-done.8.refs_1_ = bf16[128,512]{1,0:T(8,128)(2,1)S(1)} collective-permute-done((bf16[128,512]{1,0:T(8,128)(2,1)S(1)}, bf16[128,512]{1,0:T(8,128)(2,1)S(1)}, u32[]{:S(2)}, u32[]{:S(2)}) %collective-permute-start.8) | collective-permute-done | bytes 131104 | tf_op jit(solution)/shard_map/ppermute | solution.py:502
  37.0 1.3 collective-permute-done.10.refs_3_
  38.3 0.6 gather_pieces.2
  38.9 2.4 %collective-permute-start.14 = (bf16[512,512]{1,0:T(8,128)(2,1)S(1)}, bf16[512,512]{1,0:T(8,128)(2,1)S(1)}, u32[]{:S(2)}, u32[]{:S(2)}) collective-permute-start(bf16[512,512]{1,0:T(8,128)(2,1)S(1)} %bitcast.26), channel_id=1, source_target_pairs={{8,0},{10,2},{12,4},{14,6},{16,8},{18,10},{20,12},{22,14},{24,16},... | collective-permute-start | bytes 1572872 | tf_op jit(solution)/shard_map/ppermute | solution.py:506
  41.3 1.3 collective-permute-start.11
  42.6 8.4 %collective-permute-done.14.refs_13_ = bf16[512,512]{1,0:T(8,128)(2,1)S(1)} collective-permute-done((bf16[512,512]{1,0:T(8,128)(2,1)S(1)}, bf16[512,512]{1,0:T(8,128)(2,1)S(1)}, u32[]{:S(2)}, u32[]{:S(2)}) %collective-permute-start.14) | collective-permute-done | bytes 524320 | tf_op jit(solution)/shard_map/ppermute | solution.py:506
  51.0 4.4 %collective-permute-start.15 = (bf16[512,512]{1,0:T(8,128)(2,1)S(1)}, bf16[512,512]{1,0:T(8,128)(2,1)S(1)}, u32[]{:S(2)}, u32[]{:S(2)}) collective-permute-start(bf16[512,512]{1,0:T(8,128)(2,1)S(1)} %collective-permute-done.14.refs_13_), channel_id=1, source_target_pairs={{8,0},{10,2},{12,4},{14,6},{16,8},{18,10},{20,12},{22,14},{24,16},... | collective-permute-start | bytes 1572872 | tf_op jit(solution)/shard_map/ppermute | solution.py:506
  55.4 1.3 collective-permute-start.12
  56.7 1.9 slice.16
  58.6 1.5 collective-permute-start.4
  60.1 1.9 slice.17
  62.0 1.5 collective-permute-start.6
  63.5 0.7 collective-permute-done.15.refs_14_
  64.3 5.2 %collective-permute-start.16 = (bf16[512,512]{1,0:T(8,128)(2,1)S(1)}, bf16[512,512]{1,0:T(8,128)(2,1)}, u32[]{:S(2)}, u32[]{:S(2)}) collective-permute-start(bf16[512,512]{1,0:T(8,128)(2,1)S(1)} %collective-permute-done.15.refs_14_), channel_id=1, source_target_pairs={{8,0},{10,2},{12,4},{14,6},{16,8},{18,10},{20,12},{22,14},{24,16},... | collective-permute-start | bytes 1572872 | tf_op jit(solution)/shard_map/ppermute | solution.py:506
  69.5 0.5 collective-permute-start.1
  70.0 2.3 %constant_dynamic-slice_fusion.refs_16_ = bf16[2048,256]{1,0:T(8,128)(2,1)} fusion(bf16[2048,1024]{1,0:T(8,128)(2,1)} %param.9, s32[]{:T(128)S(6)} %select_n.83), kind=kLoop, calls=%fused_computation.18 | loop fusion | bytes 2097156 | tf_op jit(solution)/shard_map/dynamic_slice | solution.py:548
  72.3 1.3 collective-permute-start.13
  73.6 0.1 collective-permute-start.5
  73.7 3.0 %collective-permute-done.16.refs_15_ = bf16[512,512]{1,0:T(8,128)(2,1)} collective-permute-done((bf16[512,512]{1,0:T(8,128)(2,1)S(1)}, bf16[512,512]{1,0:T(8,128)(2,1)}, u32[]{:S(2)}, u32[]{:S(2)}) %collective-permute-start.16) | collective-permute-done | bytes 524320 | tf_op jit(solution)/shard_map/ppermute | solution.py:506
  76.7 0.1 reshape.97
  76.8 5.6 %fusion = (f32[2048,128]{1,0:T(8,128)}, f32[2048,128]{1,0:T(8,128)}) fusion(f32[128]{0:T(128)S(1)} %get-tuple-element.42, f32[128]{0:T(128)S(1)} %get-tuple-element.43, f32[2048]{0:T(1024)S(1)} %reshape.97), kind=kLoop, calls=%fused_computation.2 | loop fusion | flops 524288 | bytes 2106368 | tf_op jit(solution)/shard_map/mul | solution.py:546
  82.4 5.7 %collective-permute-done.13.refs_12_ = bf16[512,512]{1,0:T(8,128)(2,1)} collective-permute-done((bf16[512,512]{1,0:T(8,128)(2,1)S(1)}, bf16[512,512]{1,0:T(8,128)(2,1)}, u32[]{:S(2)}, u32[]{:S(2)}) %collective-permute-start.13) | collective-permute-done | bytes 524320 | tf_op jit(solution)/shard_map/ppermute | solution.py:506
  88.1 14.2 %project.1 = (bf16[2048,256]{1,0:T(8,128)(2,1)}, bf16[16,128,256]{2,1,0:T(8,128)(2,1)}, bf16[2048,256]{1,0:T(8,128)(2,1)}, bf16[2048,256]{1,0:T(8,128)(2,1)}, bf16[2,16,128,256]{3,2,1,0:T(8,128)(2,1)}) custom-call(s32[3]{0:T(128)S(1)} %pad_add_fusion.idx, bf16[512,2048]{1,0:T(8,128)(2,1)} %copy-done, bf16[256,2048]{1,0:T(8,128)(2,1)} %collective-permute-done.refs_1_, ...), custom_call_target="tpu_custom_call" | custom-call | tf_op jit(solution)/shard_map/project/pallas_call | solution.py:152
  102.3 1.5 collective-permute-start.17
  103.8 1.2 copy-done.2
  105.0 1.2 copy-done.4
  106.2 1.6 copy-done.6
  107.8 1.2 copy-done.8
  109.1 1.2 copy-done.9
  110.3 24.8 %attend_local.1 = (f32[16,16,8,256]{3,2,1,0:T(8,128)S(1)}, f32[16,16,8,256]{3,2,1,0:T(8,128)S(1)}, f32[16,16,8,256]{3,2,1,0:T(8,128)S(1)}) custom-call(bf16[2048,256]{1,0:T(8,128)(2,1)S(1)} %copy-done.2, bf16[16,128,256]{2,1,0:T(8,128)(2,1)S(1)} %copy-done.4, bf16[2048,256]{1,0:T(8,128)(2,1)S(1)} %copy-done.8, bf16[2048,256]{1,0:T(8,128)(2,1)S(1)} %copy-done.9, ...), custom_call_target="tpu_custom_call" | custom-call | tf_op jit(solution)/shard_map/attend_local/pallas_call | solution.py:325
  135.1 16.0 %collective-permute-done.17.halo = bf16[2,16,128,256]{3,2,1,0:T(8,128)(2,1)S(1)} collective-permute-done((bf16[2,16,128,256]{3,2,1,0:T(8,128)(2,1)}, bf16[2,16,128,256]{3,2,1,0:T(8,128)(2,1)S(1)}, u32[]{:S(2)}, u32[]{:S(2)}) %collective-permute-start.17) | collective-permute-done | bytes 2097184 | tf_op jit(solution)/shard_map/ppermute | solution.py:506
  151.1 12.5 %attend_halo.1 = (bf16[4,512,256]{2,1,0:T(8,128)(2,1)S(1)}, f32[4,4,512]{2,1,0:T(4,128)S(1)}) custom-call(s32[3]{0:T(128)S(1)} %pad_add_fusion.idx, bf16[2048,256]{1,0:T(8,128)(2,1)S(1)} %copy-done.3, bf16[16,128,256]{2,1,0:T(8,128)(2,1)S(1)} %copy-done.5, bf16[2,16,128,256]{3,2,1,0:T(8,128)(2,1)S(1)} %collective-permute-done.17.halo, ...), custom_call_target="tpu_custom_call" | custom-call | tf_op jit(solution)/shard_map/attend_halo/pallas_call | solution.py:410
  163.5 0.1 dynamic-slice_bitcast_fusion
  163.6 2.5 %collective-permute-start.20 = (bf16[512,256]{1,0:T(8,128)(2,1)S(1)}, bf16[512,256]{1,0:T(8,128)(2,1)S(1)}, u32[]{:S(2)}, u32[]{:S(2)}) collective-permute-start(bf16[512,256]{1,0:T(8,128)(2,1)S(1)} %get-tuple-element.24), channel_id=1, source_target_pairs={{0,6},{2,4},{4,2},{6,0},{8,14},{10,12},{12,10},{14,8},{16,22},{18,... | collective-permute-start | bytes 786440 | tf_op jit(solution)/shard_map/ppermute | solution.py:502
  166.1 0.5 collective-permute-start.19
  166.7 0.5 collective-permute-start.18
  167.2 6.6 %collective-permute-done.20.refs_3_ = bf16[512,256]{1,0:T(8,128)(2,1)S(1)} collective-permute-done((bf16[512,256]{1,0:T(8,128)(2,1)S(1)}, bf16[512,256]{1,0:T(8,128)(2,1)S(1)}, u32[]{:S(2)}, u32[]{:S(2)}) %collective-permute-start.20) | collective-permute-done | bytes 262176 | tf_op jit(solution)/shard_map/ppermute | solution.py:502
  173.8 2.9 %collective-permute-done.19.refs_2_ = bf16[512,256]{1,0:T(8,128)(2,1)S(1)} collective-permute-done((bf16[512,256]{1,0:T(8,128)(2,1)S(1)}, bf16[512,256]{1,0:T(8,128)(2,1)S(1)}, u32[]{:S(2)}, u32[]{:S(2)}) %collective-permute-start.19) | collective-permute-done | bytes 262176 | tf_op jit(solution)/shard_map/ppermute | solution.py:502
  176.7 0.1 collective-permute-done.18.refs_1_
  176.8 3.8 %out_partials.1 = bf16[2,256,2048]{2,1,0:T(8,128)(2,1)S(1)} custom-call(s32[3]{0:T(128)S(1)} %pad_add_fusion.idx, bf16[512,256]{1,0:T(8,128)(2,1)S(1)} %get-tuple-element.27.refs_0_, bf16[512,256]{1,0:T(8,128)(2,1)S(1)} %collective-permute-done.18.refs_1_, bf16[512,256]{1,0:T(8,128)(2,1)S(1)} %collective-permute-done.19.refs_2_, ...), custom_call_target="tpu_custom_call" | custom-call | tf_op jit(solution)/shard_map/out_partials/pallas_call | solution.py:450
  180.6 1.2 slice_bitcast_fusion
  181.8 1.7 collective-permute-start.24
  183.5 1.3 collective-permute-start.23
  184.8 0.6 collective-permute-start.22
  185.4 1.1 collective-permute-done.24.refs_3_
  186.5 0.7 collective-permute-done.23.refs_2_
  187.2 1.3 collective-permute-done.22.refs_1_
  188.5 0.5 gather_pieces.3
  189.0 0.6 reshape.96
  189.6 1.5 final_norm.1
  (40 shorter events, 0.1 us)
Async XLA Ops:
  0.6 1.6 copy-start.7
  2.2 0.7 copy-start.10
  5.3 8.0 %copy-start = (bf16[512,2048]{1,0:T(8,128)(2,1)}, bf16[512,2048]{1,0:T(8,128)(2,1)S(1)}, u32[]{:S(2)}) copy-start(bf16[512,2048]{1,0:T(8,128)(2,1)S(1)} %norm_rows.1.refs_0_) | copy-start | bytes 6291460
  5.3 4.1 %copy-start.12 = (bf16[128,1024]{1,0:T(8,128)(2,1)S(1)}, bf16[128,1024]{1,0:T(8,128)(2,1)}, u32[]{:S(2)}) copy-start(bf16[128,1024]{1,0:T(8,128)(2,1)} %param.11) | copy-start | bytes 786436
  5.3 4.1 %copy-start.13 = (bf16[128,1024]{1,0:T(8,128)(2,1)S(1)}, bf16[128,1024]{1,0:T(8,128)(2,1)}, u32[]{:S(2)}) copy-start(bf16[128,1024]{1,0:T(8,128)(2,1)} %param.10) | copy-start | bytes 786436
  6.4 50.3 %collective-permute-start.2 = (bf16[256,2048]{1,0:T(8,128)(2,1)}, bf16[256,2048]{1,0:T(8,128)(2,1)}, u32[]{:S(2)}, u32[]{:S(2)}) collective-permute-start(bf16[256,2048]{1,0:T(8,128)(2,1)} %constant_dynamic-slice_fusion.9), channel_id=1, source_target_pairs={{0,4},{2,6},{4,0},{6,2},{8,12},{10,14},{12,8},{14,10},{16,20},{18,... | collective-permute-start | bytes 3145736 | tf_op jit(solution)/shard_map/ppermute | solution.py:502
  7.9 52.2 %collective-permute-start = (bf16[256,2048]{1,0:T(8,128)(2,1)}, bf16[256,2048]{1,0:T(8,128)(2,1)}, u32[]{:S(2)}, u32[]{:S(2)}) collective-permute-start(bf16[256,2048]{1,0:T(8,128)(2,1)} %constant_dynamic-slice_fusion.9), channel_id=1, source_target_pairs={{0,2},{2,0},{4,6},{6,4},{8,10},{10,8},{12,14},{14,12},{16,18},{18,... | collective-permute-start | bytes 3145736 | tf_op jit(solution)/shard_map/ppermute | solution.py:502
  9.5 25.0 %collective-permute-start.9 = (bf16[128,512]{1,0:T(8,128)(2,1)S(1)}, bf16[128,512]{1,0:T(8,128)(2,1)S(1)}, u32[]{:S(2)}, u32[]{:S(2)}) collective-permute-start(bf16[128,512]{1,0:T(8,128)(2,1)S(1)} %pad_maximum_fusion.2), channel_id=1, source_target_pairs={{0,4},{2,6},{4,0},{6,2},{8,12},{10,14},{12,8},{14,10},{16,20},{18,... | collective-permute-start | bytes 393224 | tf_op jit(solution)/shard_map/ppermute | solution.py:502
  10.1 26.9 %collective-permute-start.8 = (bf16[128,512]{1,0:T(8,128)(2,1)S(1)}, bf16[128,512]{1,0:T(8,128)(2,1)S(1)}, u32[]{:S(2)}, u32[]{:S(2)}) collective-permute-start(bf16[128,512]{1,0:T(8,128)(2,1)S(1)} %pad_maximum_fusion.1), channel_id=1, source_target_pairs={{0,2},{2,0},{4,6},{6,4},{8,10},{10,8},{12,14},{14,12},{16,18},{18,... | collective-permute-start | bytes 393224 | tf_op jit(solution)/shard_map/ppermute | solution.py:502
  10.7 27.6 %collective-permute-start.10 = (bf16[128,512]{1,0:T(8,128)(2,1)S(1)}, bf16[128,512]{1,0:T(8,128)(2,1)S(1)}, u32[]{:S(2)}, u32[]{:S(2)}) collective-permute-start(bf16[128,512]{1,0:T(8,128)(2,1)S(1)} %pad_maximum_fusion.3), channel_id=1, source_target_pairs={{0,6},{2,4},{4,2},{6,0},{8,14},{10,12},{12,10},{14,8},{16,22},{18,... | collective-permute-start | bytes 393224 | tf_op jit(solution)/shard_map/ppermute | solution.py:502
  38.9 12.1 %collective-permute-start.14 = (bf16[512,512]{1,0:T(8,128)(2,1)S(1)}, bf16[512,512]{1,0:T(8,128)(2,1)S(1)}, u32[]{:S(2)}, u32[]{:S(2)}) collective-permute-start(bf16[512,512]{1,0:T(8,128)(2,1)S(1)} %bitcast.26), channel_id=1, source_target_pairs={{8,0},{10,2},{12,4},{14,6},{16,8},{18,10},{20,12},{22,14},{24,16},... | collective-permute-start | bytes 1572872 | tf_op jit(solution)/shard_map/ppermute | solution.py:506
  41.3 14.1 %collective-permute-start.11 = (bf16[512,512]{1,0:T(8,128)(2,1)S(1)}, bf16[512,512]{1,0:T(8,128)(2,1)S(1)}, u32[]{:S(2)}, u32[]{:S(2)}) collective-permute-start(bf16[512,512]{1,0:T(8,128)(2,1)S(1)} %bitcast.27), channel_id=1, source_target_pairs={{0,8},{2,10},{4,12},{6,14},{8,16},{10,18},{12,20},{14,22},{16,24},... | collective-permute-start | bytes 1572872 | tf_op jit(solution)/shard_map/ppermute | solution.py:506
  51.0 13.3 %collective-permute-start.15 = (bf16[512,512]{1,0:T(8,128)(2,1)S(1)}, bf16[512,512]{1,0:T(8,128)(2,1)S(1)}, u32[]{:S(2)}, u32[]{:S(2)}) collective-permute-start(bf16[512,512]{1,0:T(8,128)(2,1)S(1)} %collective-permute-done.14.refs_13_), channel_id=1, source_target_pairs={{8,0},{10,2},{12,4},{14,6},{16,8},{18,10},{20,12},{22,14},{24,16},... | collective-permute-start | bytes 1572872 | tf_op jit(solution)/shard_map/ppermute | solution.py:506
  55.4 14.0 %collective-permute-start.12 = (bf16[512,512]{1,0:T(8,128)(2,1)S(1)}, bf16[512,512]{1,0:T(8,128)(2,1)S(1)}, u32[]{:S(2)}, u32[]{:S(2)}) collective-permute-start(bf16[512,512]{1,0:T(8,128)(2,1)S(1)} %collective-permute-done.11.refs_10_), channel_id=1, source_target_pairs={{0,8},{2,10},{4,12},{6,14},{8,16},{10,18},{12,20},{14,22},{16,24},... | collective-permute-start | bytes 1572872 | tf_op jit(solution)/shard_map/ppermute | solution.py:506
  58.6 13.7 %collective-permute-start.4 = (bf16[128,2048]{1,0:T(8,128)(2,1)}, bf16[128,2048]{1,0:T(8,128)(2,1)S(1)}, u32[]{:S(2)}, u32[]{:S(2)}) collective-permute-start(bf16[128,2048]{1,0:T(8,128)(2,1)} %slice.16), channel_id=1, source_target_pairs={{0,2},{2,0},{4,6},{6,4},{8,10},{10,8},{12,14},{14,12},{16,18},{18,... | collective-permute-start | bytes 1572872 | tf_op jit(solution)/shard_map/ppermute | solution.py:502
  62.0 11.5 %collective-permute-start.6 = (bf16[128,2048]{1,0:T(8,128)(2,1)}, bf16[128,2048]{1,0:T(8,128)(2,1)}, u32[]{:S(2)}, u32[]{:S(2)}) collective-permute-start(bf16[128,2048]{1,0:T(8,128)(2,1)} %slice.17), channel_id=1, source_target_pairs={{0,4},{2,6},{4,0},{6,2},{8,12},{10,14},{12,8},{14,10},{16,20},{18,... | collective-permute-start | bytes 1572872 | tf_op jit(solution)/shard_map/ppermute | solution.py:502
  64.3 12.4 %collective-permute-start.16 = (bf16[512,512]{1,0:T(8,128)(2,1)S(1)}, bf16[512,512]{1,0:T(8,128)(2,1)}, u32[]{:S(2)}, u32[]{:S(2)}) collective-permute-start(bf16[512,512]{1,0:T(8,128)(2,1)S(1)} %collective-permute-done.15.refs_14_), channel_id=1, source_target_pairs={{8,0},{10,2},{12,4},{14,6},{16,8},{18,10},{20,12},{22,14},{24,16},... | collective-permute-start | bytes 1572872 | tf_op jit(solution)/shard_map/ppermute | solution.py:506
  69.5 18.6 %collective-permute-start.3 = (bf16[256,2048]{1,0:T(8,128)(2,1)}, bf16[256,2048]{1,0:T(8,128)(2,1)}, u32[]{:S(2)}, u32[]{:S(2)}) collective-permute-start(bf16[256,2048]{1,0:T(8,128)(2,1)} %collective-permute-done.2.refs_3_), channel_id=1, source_target_pairs={{0,1},{1,0},{2,3},{3,2},{4,5},{5,4},{6,7},{7,6},{8,9},{9,8},{10,11... | collective-permute-start | bytes 3145736 | tf_op jit(solution)/shard_map/ppermute | solution.py:509
  69.5 18.6 %collective-permute-start.1 = (bf16[256,2048]{1,0:T(8,128)(2,1)}, bf16[256,2048]{1,0:T(8,128)(2,1)}, u32[]{:S(2)}, u32[]{:S(2)}) collective-permute-start(bf16[256,2048]{1,0:T(8,128)(2,1)} %collective-permute-done.refs_1_), channel_id=1, source_target_pairs={{0,1},{1,0},{2,3},{3,2},{4,5},{5,4},{6,7},{7,6},{8,9},{9,8},{10,11... | collective-permute-start | bytes 3145736 | tf_op jit(solution)/shard_map/ppermute | solution.py:509
  72.3 15.8 %collective-permute-start.13 = (bf16[512,512]{1,0:T(8,128)(2,1)S(1)}, bf16[512,512]{1,0:T(8,128)(2,1)}, u32[]{:S(2)}, u32[]{:S(2)}) collective-permute-start(bf16[512,512]{1,0:T(8,128)(2,1)S(1)} %collective-permute-done.12.refs_11_), channel_id=1, source_target_pairs={{0,8},{2,10},{4,12},{6,14},{8,16},{10,18},{12,20},{14,22},{16,24},... | collective-permute-start | bytes 1572872 | tf_op jit(solution)/shard_map/ppermute | solution.py:506
  73.6 14.5 %collective-permute-start.5 = (bf16[128,2048]{1,0:T(8,128)(2,1)S(1)}, bf16[128,2048]{1,0:T(8,128)(2,1)}, u32[]{:S(2)}, u32[]{:S(2)}) collective-permute-start(bf16[128,2048]{1,0:T(8,128)(2,1)S(1)} %collective-permute-done.4.refs_5_), channel_id=1, source_target_pairs={{0,1},{1,0},{2,3},{3,2},{4,5},{5,4},{6,7},{7,6},{8,9},{9,8},{10,11... | collective-permute-start | bytes 1572872 | tf_op jit(solution)/shard_map/ppermute | solution.py:509
  76.7 11.4 %collective-permute-start.7 = (bf16[128,2048]{1,0:T(8,128)(2,1)}, bf16[128,2048]{1,0:T(8,128)(2,1)}, u32[]{:S(2)}, u32[]{:S(2)}) collective-permute-start(bf16[128,2048]{1,0:T(8,128)(2,1)} %collective-permute-done.6.refs_7_), channel_id=1, source_target_pairs={{0,1},{1,0},{2,3},{3,2},{4,5},{5,4},{6,7},{7,6},{8,9},{9,8},{10,11... | collective-permute-start | bytes 1572872 | tf_op jit(solution)/shard_map/ppermute | solution.py:509
  102.3 48.8 %collective-permute-start.17 = (bf16[2,16,128,256]{3,2,1,0:T(8,128)(2,1)}, bf16[2,16,128,256]{3,2,1,0:T(8,128)(2,1)S(1)}, u32[]{:S(2)}, u32[]{:S(2)}) collective-permute-start(bf16[2,16,128,256]{3,2,1,0:T(8,128)(2,1)} %get-tuple-element.14.kvr), channel_id=1, source_target_pairs={{0,8},{2,10},{4,12},{6,14},{8,16},{10,18},{12,20},{14,22},{16,24},... | collective-permute-start | bytes 6291464 | tf_op jit(solution)/shard_map/ppermute | solution.py:506
  103.8 1.2 copy-start.2
  105.0 1.2 copy-start.4
  106.2 1.6 copy-start.6
  107.8 1.2 copy-start.8
  109.1 1.2 copy-start.9
  110.3 40.8 %copy-start.3 = (bf16[2048,256]{1,0:T(8,128)(2,1)S(1)}, bf16[2048,256]{1,0:T(8,128)(2,1)}, u32[]{:S(2)}) copy-start(bf16[2048,256]{1,0:T(8,128)(2,1)} %get-tuple-element.12.q1) | copy-start | bytes 3145732
  110.3 40.8 %copy-start.5 = (bf16[16,128,256]{2,1,0:T(8,128)(2,1)S(1)}, bf16[16,128,256]{2,1,0:T(8,128)(2,1)}, u32[]{:S(2)}) copy-start(bf16[16,128,256]{2,1,0:T(8,128)(2,1)} %get-tuple-element.13.qr) | copy-start | bytes 3145732
  151.1 25.7 %copy-start.1 = (bf16[1024,2048]{1,0:T(8,128)(2,1)S(1)}, bf16[1024,2048]{1,0:T(8,128)(2,1)}, u32[]{:S(2)}) copy-start(bf16[1024,2048]{1,0:T(8,128)(2,1)} %refs_4_.1) | copy-start | bytes 12582916
  163.6 10.2 %collective-permute-start.20 = (bf16[512,256]{1,0:T(8,128)(2,1)S(1)}, bf16[512,256]{1,0:T(8,128)(2,1)S(1)}, u32[]{:S(2)}, u32[]{:S(2)}) collective-permute-start(bf16[512,256]{1,0:T(8,128)(2,1)S(1)} %get-tuple-element.24), channel_id=1, source_target_pairs={{0,6},{2,4},{4,2},{6,0},{8,14},{10,12},{12,10},{14,8},{16,22},{18,... | collective-permute-start | bytes 786440 | tf_op jit(solution)/shard_map/ppermute | solution.py:502
  166.1 10.6 %collective-permute-start.19 = (bf16[512,256]{1,0:T(8,128)(2,1)S(1)}, bf16[512,256]{1,0:T(8,128)(2,1)S(1)}, u32[]{:S(2)}, u32[]{:S(2)}) collective-permute-start(bf16[512,256]{1,0:T(8,128)(2,1)S(1)} %get-tuple-element.25), channel_id=1, source_target_pairs={{0,4},{2,6},{4,0},{6,2},{8,12},{10,14},{12,8},{14,10},{16,20},{18,... | collective-permute-start | bytes 786440 | tf_op jit(solution)/shard_map/ppermute | solution.py:502
  166.7 10.1 %collective-permute-start.18 = (bf16[512,256]{1,0:T(8,128)(2,1)S(1)}, bf16[512,256]{1,0:T(8,128)(2,1)S(1)}, u32[]{:S(2)}, u32[]{:S(2)}) collective-permute-start(bf16[512,256]{1,0:T(8,128)(2,1)S(1)} %get-tuple-element.26), channel_id=1, source_target_pairs={{0,2},{2,0},{4,6},{6,4},{8,10},{10,8},{12,14},{14,12},{16,18},{18,... | collective-permute-start | bytes 786440 | tf_op jit(solution)/shard_map/ppermute | solution.py:502
  180.6 9.0 %copy-start.11 = (f32[2048]{0:T(1024)S(1)}, f32[2048]{0:T(1024)}, u32[]{:S(2)}) copy-start(f32[2048]{0:T(1024)} %param.13) | copy-start | bytes 24580
  181.8 7.8 %collective-permute-start.21 = (bf16[256,2048]{1,0:T(8,128)(2,1)}, bf16[256,2048]{1,0:T(8,128)(2,1)S(1)}, u32[]{:S(2)}, u32[]{:S(2)}) collective-permute-start(bf16[256,2048]{1,0:T(8,128)(2,1)} %get-tuple-element.22), channel_id=1, source_target_pairs={{0,1},{1,0},{2,3},{3,2},{4,5},{5,4},{6,7},{7,6},{8,9},{9,8},{10,11... | collective-permute-start | bytes 3145736 | tf_op jit(solution)/shard_map/ppermute | solution.py:509
  181.8 4.7 %collective-permute-start.24 = (f32[4,512]{1,0:T(4,128)S(1)}, f32[4,512]{1,0:T(4,128)S(1)}, u32[]{:S(2)}, u32[]{:S(2)}) collective-permute-start(f32[4,512]{1,0:T(4,128)S(1)} %get-tuple-element.36), channel_id=1, source_target_pairs={{0,6},{2,4},{4,2},{6,0},{8,14},{10,12},{12,10},{14,8},{16,22},{18,... | collective-permute-start | bytes 24584 | tf_op jit(solution)/shard_map/ppermute | solution.py:502
  183.5 3.7 %collective-permute-start.23 = (f32[4,512]{1,0:T(4,128)S(1)}, f32[4,512]{1,0:T(4,128)S(1)}, u32[]{:S(2)}, u32[]{:S(2)}) collective-permute-start(f32[4,512]{1,0:T(4,128)S(1)} %get-tuple-element.37), channel_id=1, source_target_pairs={{0,4},{2,6},{4,0},{6,2},{8,12},{10,14},{12,8},{14,10},{16,20},{18,... | collective-permute-start | bytes 24584 | tf_op jit(solution)/shard_map/ppermute | solution.py:502
  184.8 3.7 %collective-permute-start.22 = (f32[4,512]{1,0:T(4,128)S(1)}, f32[4,512]{1,0:T(4,128)S(1)}, u32[]{:S(2)}, u32[]{:S(2)}) collective-permute-start(f32[4,512]{1,0:T(4,128)S(1)} %get-tuple-element.38), channel_id=1, source_target_pairs={{0,2},{2,0},{4,6},{6,4},{8,10},{10,8},{12,14},{14,12},{16,18},{18,... | collective-permute-start | bytes 24584 | tf_op jit(solution)/shard_map/ppermute | solution.py:502
